TPU v7x, 32 devices: a whole 2x2x4 slice. The times are simulated.
32 devices in a mesh: sp: 8 (over z, y), tp: 4 (over x, core).
Axes of the slice: x: 2, y: 2, z: 4, core: 2. Of those that a mesh axis runs over, the one named last changes fastest.
Arguments:
- latent: bfloat16 [4096, 4096], P(('sp', 'tp')), may hold values from -3 to 3
- context: bfloat16 [1024, 4096], P('sp'), may hold values from -6 to 6
- cond: float32 [4096], replicated, may hold values from -6 to 6
- ctx_cond: float32 [4096], replicated, may hold values from -6 to 6
- w_shift: bfloat16 [4096, 4096], P('sp', 'tp'), may hold values from -0.1875 to 0.1875
- w_scale: bfloat16 [4096, 4096], P('sp', 'tp'), may hold values from -0.09375 to 0.15478516
- w_gate: bfloat16 [4096, 4096], P('sp', 'tp'), may hold values from -0.1875 to 0.1875
- w_query: bfloat16 [4096, 2048], P(None, 'tp'), may hold values from -0.09375 to 0.09375
- key_weight: bfloat16 [4096, 1024], P(None, 'tp'), may hold values from -0.09375 to 0.09375
- value_weight: bfloat16 [4096, 1024], P(None, 'tp'), may hold values from -0.09375 to 0.09375
- w_out: bfloat16 [2048, 4096], P('tp'), may hold values from -0.125 to 0.125
- sink: float32 [16], replicated, may hold values from 4 to 8
Outputs:
- mixed: bfloat16 [4096, 4096], P(('sp', 'tp'))
All inputs are finite; a program needn't handle non-finite values.
Results may differ from a plain program's by a relative error of at most 0.035.
Values may be sent and summed in bfloat16 or wider, within the bound.
A program may use at most 64 MiB of HBM per device.

v0:
```python
import functools
import math

import jax
import jax.numpy as jnp
from jax import lax
from jax.experimental import pallas as pl
from jax.experimental.pallas import tpu as pltpu
from jax.sharding import PartitionSpec as P

HEAD = 128
SIDE = 128
GRID_WIDTH = 64
EPS = 1e-05
THETA = 10000.0
MASKED = -1e30
LOG2E = math.log2(math.e)
MESH = pl.DeviceIdType.MESH
F32 = jnp.float32
BF16 = jnp.bfloat16
CUTS = 2
TILES = 4
CORES = 2


def body(
    nsp, ntp,
    lat, ctx, cond, ctx_cond, w_shift, w_scale, w_gate, w_q, w_k, w_v, w_o, sink,
    out,
    cos_t, sin_t, st_mean, st_rstd, tslots,
    wmod, wq, wk, wv, wo, latb, ctxb, mb, part, mgath, mod, ctxkv, q_s, kv, att,
    stage, prcv, comb, xrcv,
    load_sem, msend, mrecv, tsend, trecv, lsend, lrecv, fsend, frecv, psend, precv,
    csend, crecv, hsend, hrecv, dsend, drecv, xsend, xrecv,
):
    nx = ntp // CORES
    sp = lax.axis_index("sp")
    tp = lax.axis_index("tp")
    x = lax.div(tp, CORES)
    c = lax.rem(tp, CORES)
    oc = 1 - c
    rows, width = lat.shape
    crows = ctx.shape[0]
    cut = rows // CUTS
    tokens = rows * ntp
    mcols = w_shift.shape[1]
    qc = w_q.shape[1]
    kc = w_k.shape[1]
    kv_heads = kc // HEAD
    group = qc // kc

    def at_tp(t):
        return (sp, t)

    def at_sp(s):
        return (s, tp)

    partner = at_tp(x * CORES + oc)

    def remote(src, dst, ss, rs, dev):
        return pltpu.make_async_remote_copy(
            src_ref=src, dst_ref=dst, send_sem=ss, recv_sem=rs, device_id=dev, device_id_type=MESH
        )

    loads = [
        pltpu.make_async_copy(s, d, load_sem.at[i])
        for i, (s, d) in enumerate(
            [
                (w_shift, wmod.at[0]), (w_scale, wmod.at[1]), (w_gate, wmod.at[2]),
                (ctx, ctxb), (w_k, wk), (w_v, wv), (w_q, wq),
                (lat, latb.at[tp]), (w_o, wo),
            ]
        )
    ]
    for load in loads[:3]:
        load.start()

    barrier = pltpu.get_barrier_semaphore()
    for d in range(1, nsp):
        pl.semaphore_signal(barrier, inc=1, device_id=at_sp(lax.rem(sp + d, nsp)), device_id_type=MESH)
    for d in range(1, ntp):
        pl.semaphore_signal(barrier, inc=1, device_id=at_tp(lax.rem(tp + d, ntp)), device_id_type=MESH)
    pl.semaphore_wait(barrier, nsp + ntp - 2)

    def lat_copy(d, j):
        dst = lax.rem(x + d, nx) * CORES + c
        return remote(
            lat.at[pl.ds(j * cut, cut)], latb.at[tp, pl.ds(j * cut, cut)],
            lsend.at[d - 1, j], lrecv.at[d - 1, j], at_tp(dst),
        )

    def from_x(d):
        return lax.rem(x - d + nx, nx)

    def fwd_copy(d, j):
        slot = latb.at[from_x(d) * CORES + c, pl.ds(j * cut, cut)]
        return remote(slot, slot, fsend.at[d - 1, j], frecv.at[d - 1, j], partner)

    for d in range(1, nx):
        lat_copy(d, 0).start()
    own = remote(lat, latb.at[tp], psend, precv, partner)
    own.start()

    mrows = w_shift.shape[0]
    arow = pl.ds(pl.multiple_of(sp * mrows, mrows), mrows)
    a0 = jax.nn.silu(cond[arow].reshape(1, mrows)).astype(BF16).astype(F32)
    a1 = jax.nn.silu(ctx_cond[arow].reshape(1, mrows)).astype(BF16).astype(F32)
    line = lax.broadcasted_iota(jnp.int32, (8, a0.shape[1]), 0)
    line8 = lax.broadcasted_iota(jnp.int32, (8, mcols // 2), 0)
    z = jnp.zeros((8, a0.shape[1]), F32)
    a0 = jnp.broadcast_to(a0, z.shape)
    a1 = jnp.broadcast_to(a1, z.shape)
    acc = None
    for i, (r0, r1) in enumerate(((0, 1), (2, 3), (4, -1))):
        act = jnp.where(line == r0, a0, jnp.where(line == r1, a1, z)).astype(BF16)
        loads[i].wait()
        piece = jnp.dot(act, wmod[i], preferred_element_type=F32)
        acc = piece if acc is None else acc + piece
    hc = mcols // 2
    part[...] = jnp.concatenate([acc[:, :hc], acc[:, hc:]], axis=0).astype(BF16)
    mcopies = [
        remote(part, mgath.at[d - 1], msend.at[d - 1], mrecv.at[d - 1], at_sp(lax.rem(sp + d, nsp)))
        for d in range(1, nsp)
    ]
    for cp in mcopies:
        cp.start()
    for i in (3, 7, 4, 5, 6, 8):
        loads[i].start()

    def turn_tables():
        half = HEAD // 2
        lane_i = lax.broadcasted_iota(jnp.int32, (tokens, HEAD), 1)
        inner = lax.rem(lane_i, half // 2).astype(F32)
        inverse = jnp.exp(inner * (-2.0 / half * math.log(THETA)))
        pos = (lax.broadcasted_iota(jnp.int32, (tokens, HEAD), 0) + sp * tokens).astype(F32)
        grid_row = jnp.floor(pos * (1.0 / GRID_WIDTH))
        angle = jnp.where(lane_i < half, grid_row, pos - grid_row * GRID_WIDTH) * inverse
        cos_t[...] = jnp.cos(angle)
        sin_t[...] = jnp.where(lax.rem(lane_i, half) < half // 2, -1.0, 1.0) * jnp.sin(angle)

    step = 16

    def measure_rows(src, row0, st0, count):
        @pl.loop(0, count // step, unroll=2)
        def _(i):
            v = src[pl.ds(row0 + i * step, step), :].astype(F32)
            mean = jnp.mean(v, axis=-1, keepdims=True)
            v = v - mean
            var = jnp.mean(v * v, axis=-1, keepdims=True)
            st_mean[pl.ds(st0 + i * step, step), :] = jnp.broadcast_to(mean, (step, HEAD))
            st_rstd[pl.ds(st0 + i * step, step), :] = jnp.broadcast_to(lax.rsqrt(var + EPS), (step, HEAD))

    def shift_rows(src, row0, st0, dst, dst0, count, r_shift, r_scale):
        @pl.loop(0, count // step)
        def _(i):
            v = src[pl.ds(row0 + i * step, step), :].astype(F32)
            srow = pl.ds(st0 + i * step, step)
            v = (v - st_mean[srow, 0:1]) * st_rstd[srow, 0:1]
            v = v * mod[r_scale : r_scale + 1, :] + mod[r_shift : r_shift + 1, :]
            dst[pl.ds(dst0 + i * step, step), :] = v.astype(BF16)

    lat2 = latb.reshape(ntp * rows, width)
    base = pl.multiple_of(x * CORES * rows, CORES * rows)
    loads[3].wait()
    measure_rows(ctxb, 0, CORES * rows, crows)
    loads[7].wait()
    measure_rows(lat2, pl.multiple_of(tp * rows, rows), pl.multiple_of(c * rows, rows), rows)
    acc = part[...].astype(F32)
    for d in range(1, nsp):
        mcopies[d - 1].wait_recv()
        acc = acc + mgath[d - 1].astype(F32)
    tslots[tp] = acc.astype(BF16)
    tcopies = [
        remote(tslots.at[tp], tslots.at[tp], tsend.at[d - 1], trecv.at[d - 1], at_tp(lax.rem(tp + d, ntp)))
        for d in range(1, ntp)
    ]
    for cp in tcopies:
        cp.start()
    for d in range(1, nx):
        for j in range(1, CUTS):
            lat_copy(d, j).start()
    turn_tables()
    own.wait_recv()
    measure_rows(lat2, pl.multiple_of((x * CORES + oc) * rows, rows), pl.multiple_of(oc * rows, rows), rows)
    for cp in tcopies:
        cp.wait_recv()
    for t in range(ntp):
        v = tslots[t].astype(F32)
        bump = jnp.where((line8 == 2) | (line8 == 3), 1.0, 0.0)
        mod[:, t * mcols : t * mcols + hc] = v[0:8] + bump
        mod[:, t * mcols + hc : (t + 1) * mcols] = v[8:16] + bump
    loads[4].wait()
    loads[5].wait()

    shift_rows(ctxb, 0, CORES * rows, mb, 0, crows, 1, 3)
    crow = pl.ds(pl.multiple_of(sp * crows, crows), crows)
    cm = mb[0:crows, :]
    ctxkv[crow, 0:kc] = jnp.dot(cm, wk[...], preferred_element_type=F32).astype(BF16)
    ctxkv[crow, kc : 2 * kc] = jnp.dot(cm, wv[...], preferred_element_type=F32).astype(BF16)
    ccopies = [
        remote(ctxkv.at[crow], ctxkv.at[crow], csend.at[d - 1], crecv.at[d - 1], at_sp(lax.rem(sp + d, nsp)))
        for d in range(1, nsp)
    ]
    for cp in ccopies:
        cp.start()

    for d in range(1, nx):
        lat_copy(d, 0).wait_recv()
        fwd_copy(d, 0).start()

    lane = lax.broadcasted_iota(jnp.int32, (1, HEAD), 1)
    low = lax.rem(lane, HEAD // 2) < HEAD // 4

    def turn(v, row0, count, factor):
        v = v.astype(BF16).astype(F32)
        swapped = jnp.where(low, pltpu.roll(v, HEAD - HEAD // 4, 1), pltpu.roll(v, HEAD // 4, 1))
        r = v * cos_t[pl.ds(row0, count), :] + swapped * sin_t[pl.ds(row0, count), :]
        return (r * factor).astype(BF16)

    def project(segments):
        total = sum(n for _, n in segments)
        qf = HEAD ** (-0.5) * LOG2E
        for w, cols, kind in ((wq, qc, 0), (wk, kc, 1), (wv, kc, 2)):
            tile = min(256, cols)
            for n0 in range(0, cols, tile):
                r = jnp.dot(mb[0:total, :], w[:, n0 : n0 + tile], preferred_element_type=F32)
                off = 0
                for row0, n in segments:
                    for h in range(0, tile, HEAD):
                        v = r[off : off + n, h : h + HEAD]
                        if kind == 0:
                            q_s[pl.ds(row0, n), n0 + h : n0 + h + HEAD] = turn(v, row0, n, qf)
                        elif kind == 1:
                            kv[pl.ds(row0 + SIDE, n), n0 + h : n0 + h + HEAD] = turn(v, row0, n, 1.0)
                        else:
                            kv[pl.ds(row0 + SIDE, n), kc + n0 + h : kc + n0 + h + HEAD] = v.astype(BF16)
                    off += n

    loads[6].wait()
    shift_rows(lat2, base, 0, mb, 0, CORES * rows, 0, 2)
    project([(base, CORES * rows)])

    left = at_sp(lax.rem(sp + nsp - 1, nsp))
    right = at_sp(lax.rem(sp + 1, nsp))
    to_left = remote(kv.at[pl.ds(SIDE, SIDE)], kv.at[pl.ds(SIDE + tokens, SIDE)], hsend.at[0], hrecv.at[0], left)
    to_right = remote(kv.at[pl.ds(tokens, SIDE)], kv.at[pl.ds(0, SIDE)], hsend.at[1], hrecv.at[1], right)

    @pl.when(x == 0)
    def _():
        to_left.start()

    @pl.when(x == nx - 1)
    def _():
        to_right.start()

    for d in range(1, nx):
        for j in range(CUTS):
            if j > 0:
                lat_copy(d, j).wait_recv()
                fwd_copy(d, j).start()
            r_a = pl.multiple_of((from_x(d) * CORES + c) * rows + j * cut, cut)
            r_b = pl.multiple_of((from_x(d) * CORES + oc) * rows + j * cut, cut)
            measure_rows(lat2, r_a, 0, cut)
            shift_rows(lat2, r_a, 0, mb, 0, cut, 0, 2)
            fwd_copy(d, j).wait_recv()
            measure_rows(lat2, r_b, cut, cut)
            shift_rows(lat2, r_b, cut, mb, cut, cut, 0, 2)
            project([(r_a, cut), (r_b, cut)])

    @pl.when(x != 0)
    def _():
        to_left.start()

    @pl.when(x != nx - 1)
    def _():
        to_right.start()

    for cp in ccopies:
        cp.wait_recv()
    loads[8].wait()

    band = rows + 2 * SIDE
    key_i = lax.broadcasted_iota(jnp.int32, (rows, band), 1)
    gap = key_i - lax.broadcasted_iota(jnp.int32, (rows, band), 0)
    near = (gap >= 0) & (gap <= 2 * SIDE)

    def attend(t, u):
        r0 = pl.multiple_of(t * rows, rows)
        kpos = key_i + (sp * tokens + r0 - SIDE)
        valid = near & (kpos >= 0) & (kpos < tokens * nsp)
        bias = jnp.where(valid, 0.0, MASKED)
        bias = jnp.concatenate([bias] * group, axis=0)
        for h in range(kv_heads):
            heads = [h * group + i for i in range(group)]
            q = jnp.concatenate([q_s[pl.ds(r0, rows), j * HEAD : (j + 1) * HEAD] for j in heads], axis=0)
            kb = kv[pl.ds(r0, band), h * HEAD : (h + 1) * HEAD]
            vb = kv[pl.ds(r0, band), kc + h * HEAD : kc + (h + 1) * HEAD]
            kx = ctxkv[:, h * HEAD : (h + 1) * HEAD]
            vx = ctxkv[:, kc + h * HEAD : kc + (h + 1) * HEAD]
            dims = (((1,), (1,)), ((), ()))
            sb = lax.dot_general(q, kb, dims, preferred_element_type=F32) + bias
            sx = lax.dot_general(q, kx, dims, preferred_element_type=F32)
            snk = jnp.concatenate(
                [jnp.full((rows, 1), sink[tp * (qc // HEAD) + j], F32) for j in heads], axis=0
            ) * LOG2E
            top = jnp.maximum(
                jnp.maximum(jnp.max(sb, axis=-1, keepdims=True), jnp.max(sx, axis=-1, keepdims=True)), snk
            )
            eb = jnp.exp2(sb - top)
            ex = jnp.exp2(sx - top)
            den = jnp.sum(eb, axis=-1, keepdims=True) + jnp.sum(ex, axis=-1, keepdims=True) + jnp.exp2(snk - top)
            o = jnp.dot(eb.astype(BF16), vb, preferred_element_type=F32) + jnp.dot(
                ex.astype(BF16), vx, preferred_element_type=F32
            )
            o = (o / den).astype(BF16)
            for i, j in enumerate(heads):
                att[u, :, j * HEAD : (j + 1) * HEAD] = o[i * rows : (i + 1) * rows]

    tile_cols = width // TILES
    ntile = min(512, tile_cols)

    def cols_of(n):
        return slice(n * tile_cols, (n + 1) * tile_cols)

    def x_copy(g, n, xo):
        return remote(
            comb.at[g, n], xrcv.at[g, n], xsend.at[g, n], xrecv.at[g, n], at_tp(xo * CORES + c)
        )

    def d_copy(g, n):
        return remote(stage.at[g, 0, n], prcv.at[g, n], dsend.at[g, n], drecv.at[g, n], partner)

    def combine(g, n, xo):
        d_copy(g, n).wait_recv()
        if g < nx - 1:
            comb[g, n] = (stage[g, 1, n].astype(F32) + prcv[g, n].astype(F32)).astype(BF16)
            x_copy(g, n, xo).start()

    for g in range(nx):
        xo = lax.rem(x + 1 + g, nx)
        if g == 0:
            @pl.when(x != 0)
            def _():
                to_right.wait_recv()

            @pl.when(x != nx - 1)
            def _():
                to_left.wait_recv()
        if g == nx - 1:
            @pl.when(x == 0)
            def _():
                to_right.wait_recv()

            @pl.when(x == nx - 1)
            def _():
                to_left.wait_recv()

        @pl.loop(0, 2)
        def _(u):
            attend(xo * CORES + lax.rem(oc + u, 2), u)

        for n in range(TILES):
            for u in range(2):
                for k in range(0, tile_cols, ntile):
                    stage[g, u, n, :, k : k + ntile] = jnp.dot(
                        att[u], wo[:, n * tile_cols + k : n * tile_cols + k + ntile], preferred_element_type=F32
                    ).astype(BF16)
                if u == 0:
                    d_copy(g, n).start()
            if n > 0:
                combine(g, n - 1, xo)
        combine(g, TILES - 1, xo)

    last = nx - 1
    for n in range(TILES):
        total = stage[last, 1, n].astype(F32) + prcv[last, n].astype(F32)
        for g in range(nx - 1):
            x_copy(g, n, lax.rem(x + 1 + g, nx)).wait_recv()
            total = total + xrcv[g, n].astype(F32)
        out[:, cols_of(n)] = (latb[tp, :, cols_of(n)].astype(F32) + mod[4:5, cols_of(n)] * total).astype(BF16)

    for cp in mcopies + tcopies + ccopies + [own, to_left, to_right]:
        cp.wait_send()
    for d in range(1, nx):
        for j in range(CUTS):
            lat_copy(d, j).wait_send()
            fwd_copy(d, j).wait_send()
    for g in range(nx):
        for n in range(TILES):
            d_copy(g, n).wait_send()
            if g < nx - 1:
                x_copy(g, n, lax.rem(x + 1 + g, nx)).wait_send()


def shards(lat, ctx, cond, ctx_cond, w_shift, w_scale, w_gate, w_q, w_k, w_v, w_o, sink):
    nsp = lax.axis_size("sp")
    ntp = lax.axis_size("tp")
    nx = ntp // CORES
    rows, width = lat.shape
    crows = ctx.shape[0]
    tokens = rows * ntp
    qc = w_q.shape[1]
    kc = w_k.shape[1]
    mrows, mcols = w_shift.shape
    any_ = pl.BlockSpec(memory_space=pl.ANY)
    vmem = pl.BlockSpec(memory_space=pltpu.VMEM)
    dma = pltpu.SemaphoreType.DMA
    V = pltpu.VMEM
    return pl.pallas_call(
        functools.partial(body, nsp, ntp),
        out_shape=jax.ShapeDtypeStruct((rows, width), BF16),
        in_specs=[any_, any_, vmem, vmem] + [any_] * 7 + [pl.BlockSpec(memory_space=pltpu.SMEM)],
        out_specs=vmem,
        scratch_shapes=[
            V((tokens, HEAD), F32), V((tokens, HEAD), F32), V((CORES * rows + crows, HEAD), F32),
            V((CORES * rows + crows, HEAD), F32), V((ntp, 16, mcols // 2), BF16),
            V((3, mrows, mcols), BF16), V((width, qc), BF16), V((width, kc), BF16), V((width, kc), BF16),
            V((qc, width), BF16), V((ntp, rows, width), BF16), V((crows, width), BF16),
            V((max(CORES * rows, crows), width), BF16), V((16, mcols // 2), BF16), V((nsp - 1, 16, mcols // 2), BF16),
            V((8, width), F32), V((nsp * crows, 2 * kc), BF16), V((tokens, qc), BF16),
            V((tokens + 2 * SIDE, 2 * kc), BF16), V((2, rows, qc), BF16),
            V((nx, 2, TILES, rows, width // TILES), BF16), V((nx, TILES, rows, width // TILES), BF16),
            V((nx - 1, TILES, rows, width // TILES), BF16), V((nx - 1, TILES, rows, width // TILES), BF16),
            dma((9,)), dma((nsp - 1,)), dma((nsp - 1,)), dma((ntp - 1,)), dma((ntp - 1,)),
            dma((nx - 1, CUTS)), dma((nx - 1, CUTS)), dma((nx - 1, CUTS)), dma((nx - 1, CUTS)), dma, dma,
            dma((nsp - 1,)), dma((nsp - 1,)), dma((2,)), dma((2,)), dma((nx, TILES)), dma((nx, TILES)),
            dma((nx - 1, TILES)), dma((nx - 1, TILES)),
        ],
        compiler_params=pltpu.CompilerParams(
            collective_id=0, has_side_effects=True, vmem_limit_bytes=60 * 1024 * 1024
        ),
    )(
        lat, ctx, cond, ctx_cond,
        w_shift, w_scale, w_gate, w_q, w_k, w_v, w_o, sink,
    )


def solution(mesh):
    in_specs = (
        P(("sp", "tp"), None), P("sp", None), P(), P(), P("sp", "tp"), P("sp", "tp"), P("sp", "tp"),
        P(None, "tp"), P(None, "tp"), P(None, "tp"), P("tp", None), P(),
    )
    return jax.shard_map(
        shards, mesh=mesh, in_specs=in_specs, out_specs=P(("sp", "tp"), None), check_vma=False
    )
```

profile of v0, /device:TPU:15, one launch (start us, length us, event | category | flops | bytes accessed | tf_op | source)
XLA Modules:
  0.0 81.5 jit_solution(16162745228740196650)
XLA Ops:
  0.0 79.2 %shard_map.118 = bf16[128,4096]{1,0:T(8,128)(2,1)} custom-call(bf16[128,4096]{1,0:T(8,128)(2,1)} %lat.1, bf16[128,4096]{1,0:T(8,128)(2,1)} %ctx.1, f32[4096]{0:T(1024)} %cond.1, f32[4096]{0:T(1024)} %ctx_cond.1, bf16[512,1024]{1,0:T(8,128)(2,1)} %w_shift.1, bf16[512,1024]{1,0:T(8,128)(2,1)} %w_scale.1, bf16[512,1024]{1,0:T(8,128)(2,1)} %w_gate.1, ...), custom_call_target="tpu_custom_call" | custom-call | tf_op jit(solution)/shard_map/pallas_call | solution.py:409
  79.2 2.3 %copy.14 = bf16[128,4096]{1,0:T(8,128)(2,1)} copy(bf16[128,4096]{1,0:T(8,128)(2,1)} %shard_map.118) | data formatting | bytes 2097152
where the time goes:
time: 81.7 us; the launch traced here: 81.5 us
  Pallas kernels  79.2 us (97%)
  local copies, waits for them, and re-layouts  2.29 us (3%)
    pallas_call x1, Pallas kernels, shards(): pl.pallas_call(functools.partial(body, nsp, ntp), out_shape=jax.ShapeDtyp...  79.2 us
    unnamed x1, local copies, waits for them, and re-layouts  2.29 us

commit v1 on v0

v1 whole, which is shorter than its diff:
```python
import functools
import math

import jax
import jax.numpy as jnp
from jax import lax
from jax.experimental import pallas as pl
from jax.experimental.pallas import tpu as pltpu
from jax.sharding import PartitionSpec as P

HEAD = 128
SIDE = 128
GRID_WIDTH = 64
EPS = 1e-05
THETA = 10000.0
MASKED = -1e30
LOG2E = math.log2(math.e)
MESH = pl.DeviceIdType.MESH
F32 = jnp.float32
BF16 = jnp.bfloat16
TILES = 8
LAG = 3
CORES = 2
FIRST = 16
GROUPS = ((0, 1), (2,), (3,))


def grid_y(nsp):
    ny = math.isqrt(nsp // 2)
    return ny if ny > 0 and nsp % ny == 0 else 1


def body(
    nsp, ntp,
    lat, ctx, cond, ctx_cond, w_shift, w_scale, w_gate, w_q, w_k, w_v, w_o, sink,
    out,
    cos_t, sin_t, st_mean, st_rstd, tslots,
    wmod, wq, wk, wv, wo, latb, ctxb, mb, part, mgath, mod, ctxk, ctxv, q_s, kv, att,
    stage, prcv, comb, xrcv, condb,
    load_sem, msend, mrecv, tsend, trecv, lsend, lrecv, fsend, frecv, psend, precv,
    zsend, zrecv, ysend, yrecv, hsend, hrecv, dsend, drecv, xsend, xrecv,
):
    nx = ntp // CORES
    ny = grid_y(nsp)
    nz = nsp // ny
    sp = lax.axis_index("sp")
    tp = lax.axis_index("tp")
    x = lax.div(tp, CORES)
    c = lax.rem(tp, CORES)
    oc = 1 - c
    z = lax.div(sp, ny)
    y = lax.rem(sp, ny)
    rows, width = lat.shape
    crows = ctx.shape[0]
    tokens = rows * ntp
    mcols = w_shift.shape[1]
    nc = mcols // HEAD
    qc = w_q.shape[1]
    kc = w_k.shape[1]
    kv_heads = kc // HEAD
    group = qc // kc
    edges = [0, FIRST, rows // 2, rows // 4 * 3, rows]
    ncut = len(edges) - 1

    def at_tp(t):
        return (sp, t)

    def at_sp(s):
        return (s, tp)

    partner = at_tp(x * CORES + oc)

    def remote(src, dst, ss, rs, dev):
        return pltpu.make_async_remote_copy(
            src_ref=src, dst_ref=dst, send_sem=ss, recv_sem=rs, device_id=dev, device_id_type=MESH
        )

    loads = [
        pltpu.make_async_copy(s, d, load_sem.at[i])
        for i, (s, d) in enumerate(
            [
                (w_shift, wmod.at[0]), (w_scale, wmod.at[1]), (w_gate, wmod.at[2]),
                (ctx, ctxb), (w_k, wk), (w_v, wv), (w_q, wq),
                (lat, latb.at[tp]), (w_o, wo), (cond, condb.at[0]), (ctx_cond, condb.at[1]),
            ]
        )
    ]
    for i in (9, 10, 0, 1, 2, 7, 3):
        loads[i].start()

    barrier = pltpu.get_barrier_semaphore()
    for d in range(1, nsp):
        pl.semaphore_signal(barrier, inc=1, device_id=at_sp(lax.rem(sp + d, nsp)), device_id_type=MESH)
    for d in range(1, ntp):
        pl.semaphore_signal(barrier, inc=1, device_id=at_tp(lax.rem(tp + d, ntp)), device_id_type=MESH)

    def lat_copy(d, j):
        dst = lax.rem(x + d, nx) * CORES + c
        piece = latb.at[tp, pl.ds(edges[j], edges[j + 1] - edges[j])]
        return remote(piece, piece, lsend.at[d - 1, j], lrecv.at[d - 1, j], at_tp(dst))

    def from_x(d):
        return lax.rem(x - d + nx, nx)

    def fwd_copy(d, j):
        slot = latb.at[from_x(d) * CORES + c, pl.ds(edges[j], edges[j + 1] - edges[j])]
        return remote(slot, slot, fsend.at[d - 1, j], frecv.at[d - 1, j], partner)

    def turn_tables():
        half = HEAD // 2
        lane_i = lax.broadcasted_iota(jnp.int32, (tokens, HEAD), 1)
        inner = lax.rem(lane_i, half // 2).astype(F32)
        inverse = jnp.exp(inner * (-2.0 / half * math.log(THETA)))
        pos = (lax.broadcasted_iota(jnp.int32, (tokens, HEAD), 0) + sp * tokens).astype(F32)
        grid_row = jnp.floor(pos * (1.0 / GRID_WIDTH))
        angle = jnp.where(lane_i < half, grid_row, pos - grid_row * GRID_WIDTH) * inverse
        cos_t[...] = jnp.cos(angle)
        sin_t[...] = jnp.where(lax.rem(lane_i, half) < half // 2, -1.0, 1.0) * jnp.sin(angle)

    turn_tables()
    mrows = w_shift.shape[0]
    arow = pl.ds(pl.multiple_of(sp * mrows, mrows), mrows)
    loads[9].wait()
    loads[10].wait()
    a0 = jax.nn.silu(condb[0:1, arow]).astype(BF16).astype(F32)
    a1 = jax.nn.silu(condb[1:2, arow]).astype(BF16).astype(F32)
    line = lax.broadcasted_iota(jnp.int32, (8, mrows), 0)
    zero = jnp.zeros((8, mrows), F32)
    a0 = jnp.broadcast_to(a0, zero.shape)
    a1 = jnp.broadcast_to(a1, zero.shape)
    acc = None
    for i, (r0, r1) in enumerate(((0, 1), (2, 3), (4, -1))):
        act = jnp.where(line == r0, a0, jnp.where(line == r1, a1, zero)).astype(BF16)
        loads[i].wait()
        piece = jnp.dot(act, wmod[i], preferred_element_type=F32)
        acc = piece if acc is None else acc + piece
    for k, (r0, r1) in enumerate(((1, 3), (0, 2), (4, 4))):
        part[k] = jnp.concatenate(
            [acc[r : r + 1, i * HEAD : (i + 1) * HEAD] for r in (r0, r1) for i in range(nc)], axis=0
        ).astype(BF16)
    pl.semaphore_wait(barrier, nsp + ntp - 2)
    loads[7].wait()
    mcopies = [
        [
            remote(
                part.at[cut], mgath.at[d - 1, cut], msend.at[d - 1, e], mrecv.at[d - 1, e],
                at_sp(lax.rem(sp + d, nsp)),
            )
            for d in range(1, nsp)
        ]
        for e, cut in enumerate((pl.ds(0, 1), pl.ds(1, 2)))
    ]
    for cp in mcopies[0]:
        cp.start()
    for d in range(1, nx):
        lat_copy(d, 0).start()
    for cp in mcopies[1]:
        cp.start()
    own = remote(latb.at[tp], latb.at[tp], psend, precv, partner)
    own.start()
    for i in (4, 5, 6, 8):
        loads[i].start()

    def measure_rows(src, row0, st0, count):
        step = 16

        @pl.loop(0, count // step)
        def _(i):
            v = src[pl.ds(row0 + i * step, step), :]
            parts = [None] * 4
            for j in range(width // HEAD):
                t = v[:, j * HEAD : (j + 1) * HEAD].astype(F32)
                parts[j % 4] = t if parts[j % 4] is None else parts[j % 4] + t
            st_mean[pl.ds(st0 + i * step, step), :] = (parts[0] + parts[1]) + (parts[2] + parts[3])

        whole = pl.ds(st0, count)
        mean = jnp.sum(st_mean[whole, :], axis=-1, keepdims=True) * (1.0 / width)
        st_mean[whole, :] = jnp.broadcast_to(mean, (count, HEAD))

        @pl.loop(0, count // step)
        def _(i):
            v = src[pl.ds(row0 + i * step, step), :]
            m = st_mean[pl.ds(st0 + i * step, step), :]
            parts = [None] * 4
            for j in range(width // HEAD):
                t = v[:, j * HEAD : (j + 1) * HEAD].astype(F32) - m
                t = t * t
                parts[j % 4] = t if parts[j % 4] is None else parts[j % 4] + t
            st_rstd[pl.ds(st0 + i * step, step), :] = (parts[0] + parts[1]) + (parts[2] + parts[3])

        var = jnp.sum(st_rstd[whole, :], axis=-1, keepdims=True) * (1.0 / width)
        st_rstd[whole, :] = jnp.broadcast_to(lax.rsqrt(var + EPS), (count, HEAD))

    def shift_rows(src, row0, st0, dst, dst0, count, r_shift, r_scale):
        step = min(32, count)
        rep = step // 8

        @pl.loop(0, count // step)
        def _(i):
            srow = pl.ds(st0 + i * step, step)
            m = st_mean[srow, :]
            r = st_rstd[srow, :]
            for j in range(width // HEAD):
                cols = slice(j * HEAD, (j + 1) * HEAD)
                v = src[pl.ds(row0 + i * step, step), cols].astype(F32)
                v = (v - m) * r
                sc = jnp.concatenate([mod[r_scale, :, cols]] * rep, axis=0)
                sh = jnp.concatenate([mod[r_shift, :, cols]] * rep, axis=0)
                dst[pl.ds(dst0 + i * step, step), cols] = (v * sc + sh).astype(BF16)

    lat2 = latb.reshape(ntp * rows, width)
    base = pl.multiple_of(x * CORES * rows, CORES * rows)
    measure_rows(lat2, pl.multiple_of(tp * rows, rows), pl.multiple_of(c * rows, rows), rows)
    loads[3].wait()
    measure_rows(ctxb, 0, CORES * rows, crows)
    tcopies = [
        [
            remote(
                tslots.at[tp, cut], tslots.at[tp, cut], tsend.at[d - 1, e], trecv.at[d - 1, e],
                at_tp(lax.rem(tp + d, ntp)),
            )
            for d in range(1, ntp)
        ]
        for e, cut in enumerate((pl.ds(0, 1), pl.ds(1, 2)))
    ]
    for e, cut in enumerate((slice(0, 1), slice(1, 3))):
        acc = part[cut].astype(F32)
        for d in range(1, nsp):
            mcopies[e][d - 1].wait_recv()
            acc = acc + mgath[d - 1, cut].astype(F32)
        tslots[tp, cut] = acc.astype(BF16)
        for cp in tcopies[e]:
            cp.start()
    for d in range(1, nx):
        for j in range(1, ncut):
            lat_copy(d, j).start()
    own.wait_recv()
    measure_rows(lat2, pl.multiple_of((x * CORES + oc) * rows, rows), pl.multiple_of(oc * rows, rows), rows)

    def spread(e, picks):
        for cp in tcopies[e]:
            cp.wait_recv()
        for k, first, r, bump in picks:
            for t in range(ntp):
                v = tslots[t, k].astype(F32)
                for i in range(nc):
                    row = v[first * nc + i : first * nc + i + 1] + bump
                    mod[r, :, t * mcols + i * HEAD : t * mcols + (i + 1) * HEAD] = jnp.broadcast_to(row, (8, HEAD))

    spread(0, ((0, 0, 1, 0.0), (0, 1, 3, 1.0)))
    loads[4].wait()
    loads[5].wait()

    def ctx_block(h, o):
        return (ctxk if h == 0 else ctxv).at[pl.ds(pl.multiple_of(o * crows, crows), crows)]

    def z_copy(way, k, h, o):
        to = jnp.clip(z + (1 if way == 0 else -1), 0, nz - 1) * ny + y
        return remote(ctx_block(h, o), ctx_block(h, o), zsend.at[way, k, h], zrecv.at[way, k, h], at_sp(to))

    def y_copy(d, slot, h, o):
        to = z * ny + lax.rem(y + d, ny)
        return remote(
            ctx_block(h, o), ctx_block(h, o), ysend.at[d - 1, slot, h], yrecv.at[d - 1, slot, h], at_sp(to)
        )

    def arrived(k, way):
        return (z >= k) if way == 0 else (z + k < nz)

    def goes_on(way):
        return (z + 1 < nz) if way == 0 else (z >= 1)

    def origin(k, way):
        return z - k if way == 0 else z + k

    def pass_on(k, way, h, o, act):
        if k < nz - 1:
            @pl.when(goes_on(way))
            def _():
                act(z_copy(way, k, h, o))
        if k > 0 or way == 0:
            for d in range(1, ny):
                act(y_copy(d, 2 * k - 1 + way if k > 0 else 0, h, o))

    def each_block(k, fn):
        for way in range(2):
            if k == 0:
                fn(way, sp)
            else:
                @pl.when(arrived(k, way))
                def _():
                    fn(way, origin(k, way) * ny + y)

    def relay(k, h):
        def one(way, o):
            if k > 0:
                z_copy(way, k - 1, h, o).wait_recv()
            pass_on(k, way, h, o, lambda cp: cp.start())

        each_block(k, one)

    shift_rows(ctxb, 0, CORES * rows, mb, 0, crows, 1, 3)
    crow = pl.ds(pl.multiple_of(sp * crows, crows), crows)
    for h, (w, dst) in enumerate(((wk, ctxk), (wv, ctxv))):
        dst[crow, :] = jnp.dot(mb[0:crows, :], w[...], preferred_element_type=F32).astype(BF16)
        relay(0, h)
    events = [(k, h) for k in range(1, nz) for h in range(2)]

    def poll(n):
        for _ in range(n):
            if events:
                k, h = events.pop(0)
                relay(k, h)

    spread(1, ((1, 0, 0, 0.0), (1, 1, 2, 1.0), (2, 0, 4, 0.0)))

    lane = lax.broadcasted_iota(jnp.int32, (1, HEAD), 1)
    low = lax.rem(lane, HEAD // 2) < HEAD // 4

    def turn(v, row0, count, factor):
        v = v.astype(BF16).astype(F32)
        swapped = jnp.where(low, pltpu.roll(v, HEAD - HEAD // 4, 1), pltpu.roll(v, HEAD // 4, 1))
        r = v * cos_t[pl.ds(row0, count), :] + swapped * sin_t[pl.ds(row0, count), :]
        return (r * factor).astype(BF16)

    def project(segments):
        total = sum(n for _, n in segments)
        qf = HEAD ** (-0.5) * LOG2E
        for w, cols, kind in ((wq, qc, 0), (wk, kc, 1), (wv, kc, 2)):
            tile = min(256, cols)
            for n0 in range(0, cols, tile):
                r = jnp.dot(mb[0:total, :], w[:, n0 : n0 + tile], preferred_element_type=F32)
                off = 0
                for row0, n in segments:
                    for h in range(0, tile, HEAD):
                        v = r[off : off + n, h : h + HEAD]
                        if kind == 0:
                            q_s[pl.ds(row0, n), n0 + h : n0 + h + HEAD] = turn(v, row0, n, qf)
                        elif kind == 1:
                            kv[pl.ds(row0 + SIDE, n), n0 + h : n0 + h + HEAD] = turn(v, row0, n, 1.0)
                        else:
                            kv[pl.ds(row0 + SIDE, n), kc + n0 + h : kc + n0 + h + HEAD] = v.astype(BF16)
                    off += n

    loads[6].wait()
    shift_rows(lat2, base, 0, mb, 0, CORES * rows, 0, 2)
    project([(base, CORES * rows)])
    poll(2)

    left = at_sp(lax.rem(sp + nsp - 1, nsp))
    right = at_sp(lax.rem(sp + 1, nsp))
    to_left = remote(kv.at[pl.ds(SIDE, SIDE)], kv.at[pl.ds(SIDE + tokens, SIDE)], hsend.at[0], hrecv.at[0], left)
    to_right = remote(kv.at[pl.ds(tokens, SIDE)], kv.at[pl.ds(0, SIDE)], hsend.at[1], hrecv.at[1], right)

    for d in range(1, nx):
        for g, cuts in enumerate(GROUPS):
            segments = []
            for j in cuts:
                lat_copy(d, j).wait_recv()
                fwd_copy(d, j).start()
            r0, n = edges[cuts[0]], edges[cuts[-1] + 1] - edges[cuts[0]]
            r_a = pl.multiple_of((from_x(d) * CORES + c) * rows + r0, 16)
            r_b = pl.multiple_of((from_x(d) * CORES + oc) * rows + r0, 16)
            measure_rows(lat2, r_a, 0, n)
            shift_rows(lat2, r_a, 0, mb, 0, n, 0, 2)
            for j in cuts:
                fwd_copy(d, j).wait_recv()
            measure_rows(lat2, r_b, n, n)
            shift_rows(lat2, r_b, n, mb, n, n, 0, 2)
            project([(r_a, n), (r_b, n)])
            if d == 1:
                poll(2)
                if g == 0:
                    @pl.when(x == 0)
                    def _():
                        to_left.start()

                    @pl.when(x == nx - 1)
                    def _():
                        to_right.start()
    poll(len(events))

    @pl.when(x != 0)
    def _():
        to_left.start()

    @pl.when(x != nx - 1)
    def _():
        to_right.start()


    def y_wait(k, way, h):
        for d in range(1, ny):
            o = origin(k, way) * ny + lax.rem(y - d + ny, ny)
            y_copy(d, 2 * k - 1 + way if k > 0 else 0, h, o).wait_recv()

    for h in range(2):
        y_wait(0, 0, h)
    for k in range(1, nz):
        for way in range(2):
            @pl.when(arrived(k, way))
            def _():
                for h in range(2):
                    y_wait(k, way, h)
    loads[8].wait()

    band = rows + 2 * SIDE
    key_i = lax.broadcasted_iota(jnp.int32, (rows, band), 1)
    gap = key_i - lax.broadcasted_iota(jnp.int32, (rows, band), 0)
    near = (gap >= 0) & (gap <= 2 * SIDE)

    def attend(t, u):
        r0 = pl.multiple_of(t * rows, rows)
        kpos = key_i + (sp * tokens + r0 - SIDE)
        valid = near & (kpos >= 0) & (kpos < tokens * nsp)
        bias = jnp.where(valid, 0.0, MASKED)
        bias = jnp.concatenate([bias] * group, axis=0)
        for h in range(kv_heads):
            heads = [h * group + i for i in range(group)]
            q = jnp.concatenate([q_s[pl.ds(r0, rows), j * HEAD : (j + 1) * HEAD] for j in heads], axis=0)
            kb = kv[pl.ds(r0, band), h * HEAD : (h + 1) * HEAD]
            vb = kv[pl.ds(r0, band), kc + h * HEAD : kc + (h + 1) * HEAD]
            kx = ctxk[:, h * HEAD : (h + 1) * HEAD]
            vx = ctxv[:, h * HEAD : (h + 1) * HEAD]
            dims = (((1,), (1,)), ((), ()))
            sb = lax.dot_general(q, kb, dims, preferred_element_type=F32) + bias
            sx = lax.dot_general(q, kx, dims, preferred_element_type=F32)
            snk = jnp.concatenate(
                [jnp.full((rows, 1), sink[tp * (qc // HEAD) + j], F32) for j in heads], axis=0
            ) * LOG2E
            top = jnp.maximum(
                jnp.maximum(jnp.max(sb, axis=-1, keepdims=True), jnp.max(sx, axis=-1, keepdims=True)), snk
            )
            eb = jnp.exp2(sb - top)
            ex = jnp.exp2(sx - top)
            den = jnp.sum(eb, axis=-1, keepdims=True) + jnp.sum(ex, axis=-1, keepdims=True) + jnp.exp2(snk - top)
            o = jnp.dot(eb.astype(BF16), vb, preferred_element_type=F32) + jnp.dot(
                ex.astype(BF16), vx, preferred_element_type=F32
            )
            o = (o / den).astype(BF16)
            for i, j in enumerate(heads):
                att[pl.ds(pl.multiple_of(u * rows, rows), rows), j * HEAD : (j + 1) * HEAD] = o[i * rows : (i + 1) * rows]

    tile_cols = width // TILES

    def cols_of(n):
        return slice(n * tile_cols, (n + 1) * tile_cols)

    def x_copy(g, n, xo):
        return remote(
            comb.at[g, n], xrcv.at[g, n], xsend.at[g, n], xrecv.at[g, n], at_tp(xo * CORES + c)
        )

    def d_copy(g, n):
        return remote(stage.at[g, n, pl.ds(0, rows)], prcv.at[g, n], dsend.at[g, n], drecv.at[g, n], partner)

    def combine(g, n, xo):
        d_copy(g, n).wait_recv()
        if g < nx - 1:
            comb[g, n] = (stage[g, n, rows : 2 * rows].astype(F32) + prcv[g, n].astype(F32)).astype(BF16)
            x_copy(g, n, xo).start()

    for g in range(nx):
        xo = lax.rem(x + 1 + g, nx)
        if g == 0:
            @pl.when(x != 0)
            def _():
                to_right.wait_recv()

            @pl.when(x != nx - 1)
            def _():
                to_left.wait_recv()
        if g == nx - 1:
            @pl.when(x == 0)
            def _():
                to_right.wait_recv()

            @pl.when(x == nx - 1)
            def _():
                to_left.wait_recv()


        @pl.loop(0, 2)
        def _(u):
            attend(xo * CORES + lax.rem(oc + u, 2), u)

        for n in range(TILES + LAG):
            if n < TILES:
                stage[g, n] = jnp.dot(att[...], wo[:, cols_of(n)], preferred_element_type=F32).astype(BF16)
                d_copy(g, n).start()
            if n >= LAG:
                combine(g, n - LAG, xo)

    last = nx - 1
    for n in range(TILES):
        total = stage[last, n, rows : 2 * rows].astype(F32) + prcv[last, n].astype(F32)
        for g in range(nx - 1):
            x_copy(g, n, lax.rem(x + 1 + g, nx)).wait_recv()
            total = total + xrcv[g, n].astype(F32)
        out[:, cols_of(n)] = (latb[tp, :, cols_of(n)].astype(F32) + mod[4, 0:1, cols_of(n)] * total).astype(BF16)

    for cp in mcopies[0] + mcopies[1] + tcopies[0] + tcopies[1] + [own, to_left, to_right]:
        cp.wait_send()
    for k in range(nz):
        for h in range(2):
            each_block(k, lambda way, o, k=k, h=h: pass_on(k, way, h, o, lambda cp: cp.wait_send()))
    for d in range(1, nx):
        for j in range(ncut):
            lat_copy(d, j).wait_send()
            fwd_copy(d, j).wait_send()
    for g in range(nx):
        for n in range(TILES):
            d_copy(g, n).wait_send()
            if g < nx - 1:
                x_copy(g, n, lax.rem(x + 1 + g, nx)).wait_send()


def shards(lat, ctx, cond, ctx_cond, w_shift, w_scale, w_gate, w_q, w_k, w_v, w_o, sink):
    nsp = lax.axis_size("sp")
    ntp = lax.axis_size("tp")
    nx = ntp // CORES
    ny = grid_y(nsp)
    nz = nsp // ny
    hops = max(nz - 1, 1)
    rows, width = lat.shape
    crows = ctx.shape[0]
    tokens = rows * ntp
    qc = w_q.shape[1]
    kc = w_k.shape[1]
    mrows, mcols = w_shift.shape
    nc2 = 2 * (mcols // HEAD)
    ncut = 4
    any_ = pl.BlockSpec(memory_space=pl.ANY)
    vmem = pl.BlockSpec(memory_space=pltpu.VMEM)
    dma = pltpu.SemaphoreType.DMA
    V = pltpu.VMEM
    return pl.pallas_call(
        functools.partial(body, nsp, ntp),
        out_shape=pltpu.VMEM((rows, width), BF16),
        in_specs=[any_] * 11 + [pl.BlockSpec(memory_space=pltpu.SMEM)],
        out_specs=vmem,
        scratch_shapes=[
            V((tokens, HEAD), F32), V((tokens, HEAD), F32), V((CORES * rows + crows, HEAD), F32),
            V((CORES * rows + crows, HEAD), F32), V((ntp, 3, nc2, HEAD), BF16),
            V((3, mrows, mcols), BF16), V((width, qc), BF16), V((width, kc), BF16), V((width, kc), BF16),
            V((qc, width), BF16), V((ntp, rows, width), BF16), V((crows, width), BF16),
            V((max(CORES * rows, crows), width), BF16), V((3, nc2, HEAD), BF16), V((nsp - 1, 3, nc2, HEAD), BF16),
            V((5, 8, width), F32), V((nsp * crows, kc), BF16), V((nsp * crows, kc), BF16), V((tokens, qc), BF16),
            V((tokens + 2 * SIDE, 2 * kc), BF16), V((2 * rows, qc), BF16),
            V((nx, TILES, 2 * rows, width // TILES), BF16), V((nx, TILES, rows, width // TILES), BF16),
            V((nx - 1, TILES, rows, width // TILES), BF16), V((nx - 1, TILES, rows, width // TILES), BF16),
            V((2, width), F32),
            dma((11,)), dma((nsp - 1, 2)), dma((nsp - 1, 2)), dma((ntp - 1, 2)), dma((ntp - 1, 2)),
            dma((nx - 1, ncut)), dma((nx - 1, ncut)), dma((nx - 1, ncut)), dma((nx - 1, ncut)), dma, dma,
            dma((2, hops, 2)), dma((2, hops, 2)), dma((max(ny - 1, 1), 2 * nz - 1, 2)),
            dma((max(ny - 1, 1), 2 * nz - 1, 2)), dma((2,)), dma((2,)), dma((nx, TILES)), dma((nx, TILES)),
            dma((nx - 1, TILES)), dma((nx - 1, TILES)),
        ],
        compiler_params=pltpu.CompilerParams(
            collective_id=0, has_side_effects=True, vmem_limit_bytes=60 * 1024 * 1024
        ),
    )(
        lat, ctx, cond, ctx_cond,
        w_shift, w_scale, w_gate, w_q, w_k, w_v, w_o, sink,
    )


def solution(mesh):
    in_specs = (
        P(("sp", "tp"), None), P("sp", None), P(), P(), P("sp", "tp"), P("sp", "tp"), P("sp", "tp"),
        P(None, "tp"), P(None, "tp"), P(None, "tp"), P("tp", None), P(),
    )
    return jax.shard_map(
        shards, mesh=mesh, in_specs=in_specs, out_specs=P(("sp", "tp"), None), check_vma=False
    )
```

time: 81.7 us -> 68.1 us (0.83)
  the two profiles are of different devices: /device:TPU:15 before, /device:TPU:1 now
where the time goes in v1:
time: 68.1 us; the launch traced here: 67.3 us
  Pallas kernels  66.3 us (97%)
  local copies, waits for them, and re-layouts  0.97 us (1%)
    pallas_call x1, Pallas kernels, shards(): pl.pallas_call(functools.partial(body, nsp, ntp), out_shape=pltpu.VMEM((r...  66.3 us

profile of v1, /device:TPU:1, one launch (start us, length us, event | category | flops | bytes accessed | tf_op | source)
XLA Modules:
  0.0 67.3 jit_solution(14012617410712777316)
XLA Ops:
  0.0 66.3 %shard_map.118 = bf16[128,4096]{1,0:T(8,128)(2,1)S(1)} custom-call(bf16[128,4096]{1,0:T(8,128)(2,1)} %lat.1, bf16[128,4096]{1,0:T(8,128)(2,1)} %ctx.1, f32[4096]{0:T(1024)} %cond.1, f32[4096]{0:T(1024)} %ctx_cond.1, bf16[512,1024]{1,0:T(8,128)(2,1)} %w_shift.1, bf16[512,1024]{1,0:T(8,128)(2,1)} %w_scale.1, bf16[512,1024]{1,0:T(8,128)(2,1)} %w_gate.1, ...), custom_call_target="tpu_custom_call" | custom-call | tf_op jit(solution)/shard_map/pallas_call | solution.py:537
  66.3 1.0 %copy.14 = bf16[128,4096]{1,0:T(8,128)(2,1)} copy(bf16[128,4096]{1,0:T(8,128)(2,1)S(1)} %shard_map.118) | data formatting | bytes 2097152

commit v2 on v1

v2 whole, which is shorter than its diff:
```python
import functools
import math

import jax
import jax.numpy as jnp
from jax import lax
from jax.experimental import pallas as pl
from jax.experimental.pallas import tpu as pltpu
from jax.sharding import PartitionSpec as P

HEAD = 128
SIDE = 128
GRID_WIDTH = 64
EPS = 1e-05
THETA = 10000.0
MASKED = -1e30
LOG2E = math.log2(math.e)
MESH = pl.DeviceIdType.MESH
F32 = jnp.float32
BF16 = jnp.bfloat16
UNIT = 16
TILES = 4
CORES = 2


def grid_y(nsp):
    ny = math.isqrt(nsp // 2)
    return ny if ny > 0 and nsp % ny == 0 else 1


def unit_plan(rows):
    units = rows // UNIT
    rest = [u for u in range(2 * units) if u % units]
    steps = [(0, units)] + list(zip(rest[0::2], rest[1::2]))
    fresh, used = [], 0
    for quarter in range(1, 5):
        need = 1 + max(i for i, pair in enumerate(steps) if min(pair) < quarter * units // 2)
        fresh.append(list(range(used, max(need, used))))
        used = max(need, used)
    return units, steps, fresh


def body(
    nsp, ntp,
    lat, ctx, cond, ctx_cond, w_shift, w_scale, w_gate, w_q, w_k, w_v, w_o, sink_h,
    out,
    cos_t, sin_t, st_mean, st_rstd, tslots,
    wmod, wq, wk, wv, wo, latb, ctxb, mb, part, mgath, mod, ctxk, ctxv, q_s, kv, att,
    away, keep, prcv, comb, xrcv, stage, orcv, condb, sink,
    load_sem, msend, mrecv, tsend, trecv, lsend, lrecv, fsend, frecv, psend, precv,
    zsend, zrecv, ysend, yrecv, hsend, hrecv, dsend, drecv, xsend, xrecv, osend, orecv,
):
    nx = ntp // CORES
    ny = grid_y(nsp)
    nz = nsp // ny
    sp = lax.axis_index("sp")
    tp = lax.axis_index("tp")
    x = lax.div(tp, CORES)
    c = lax.rem(tp, CORES)
    oc = 1 - c
    z = lax.div(sp, ny)
    y = lax.rem(sp, ny)
    rows, width = lat.shape
    crows = ctx.shape[0]
    tokens = rows * ntp
    mcols = w_shift.shape[1]
    nc = mcols // HEAD
    qc = w_q.shape[1]
    kc = w_k.shape[1]
    kv_heads = kc // HEAD
    group = qc // kc
    chip = CORES * rows
    units, steps, fresh = unit_plan(rows)

    def at_tp(t):
        return (sp, t)

    def at_sp(s):
        return (s, tp)

    partner = at_tp(x * CORES + oc)

    def remote(src, dst, ss, rs, dev):
        return pltpu.make_async_remote_copy(
            src_ref=src, dst_ref=dst, send_sem=ss, recv_sem=rs, device_id=dev, device_id_type=MESH
        )

    mine = pl.ds(pl.multiple_of(tp * rows, rows), rows)
    loads = [
        pltpu.make_async_copy(s, d, load_sem.at[i])
        for i, (s, d) in enumerate(
            [
                (w_shift, wmod.at[0]), (w_scale, wmod.at[1]), (w_gate, wmod.at[2]),
                (ctx, ctxb), (w_k, wk), (w_v, wv), (w_q, wq),
                (lat, latb.at[mine]), (w_o, wo), (cond, condb.at[0]), (ctx_cond, condb.at[1]), (sink_h, sink),
            ]
        )
    ]
    for i in (9, 10, 0, 1, 2, 7, 3, 11):
        loads[i].start()

    barrier = pltpu.get_barrier_semaphore()
    for d in range(1, nsp):
        pl.semaphore_signal(barrier, inc=1, device_id=at_sp(lax.rem(sp + d, nsp)), device_id_type=MESH)
    for d in range(1, ntp):
        pl.semaphore_signal(barrier, inc=1, device_id=at_tp(lax.rem(tp + d, ntp)), device_id_type=MESH)

    def from_x(d):
        return lax.rem(x - d + nx, nx)

    def chip_rows(xc, k, core):
        first, second = steps[k]
        start = xc * chip + (first + core * (second - first)) * UNIT
        return latb.at[pl.ds(pl.multiple_of(start, UNIT), UNIT)]

    def lat_copy(d, k, xc):
        dst = lax.rem(x + d, nx) * CORES + c
        return remote(chip_rows(xc, k, c), chip_rows(xc, k, c), lsend.at[d - 1], lrecv.at[d - 1, k], at_tp(dst))

    def fwd_copy(d, k, core):
        piece = chip_rows(from_x(d), k, core)
        return remote(piece, piece, fsend.at[d - 1], frecv.at[d - 1, k], partner)

    def turn_tables():
        half = HEAD // 2
        lane_i = lax.broadcasted_iota(jnp.int32, (tokens, HEAD), 1)
        inner = lax.rem(lane_i, half // 2).astype(F32)
        inverse = jnp.exp(inner * (-2.0 / half * math.log(THETA)))
        pos = (lax.broadcasted_iota(jnp.int32, (tokens, HEAD), 0) + sp * tokens).astype(F32)
        grid_row = jnp.floor(pos * (1.0 / GRID_WIDTH))
        angle = jnp.where(lane_i < half, grid_row, pos - grid_row * GRID_WIDTH) * inverse
        cos_t[...] = jnp.cos(angle)
        sin_t[...] = jnp.where(lax.rem(lane_i, half) < half // 2, -1.0, 1.0) * jnp.sin(angle)

    turn_tables()
    mrows = w_shift.shape[0]
    arow = pl.ds(pl.multiple_of(sp * mrows, mrows), mrows)
    loads[9].wait()
    loads[10].wait()
    a0 = jax.nn.silu(condb[0:1, arow]).astype(BF16).astype(F32)
    a1 = jax.nn.silu(condb[1:2, arow]).astype(BF16).astype(F32)
    line = lax.broadcasted_iota(jnp.int32, (8, mrows), 0)
    zero = jnp.zeros((8, mrows), F32)
    a0 = jnp.broadcast_to(a0, zero.shape)
    a1 = jnp.broadcast_to(a1, zero.shape)
    acc = None
    for i, (r0, r1) in enumerate(((0, 1), (2, 3), (4, -1))):
        act = jnp.where(line == r0, a0, jnp.where(line == r1, a1, zero)).astype(BF16)
        loads[i].wait()
        piece = jnp.dot(act, wmod[i], preferred_element_type=F32)
        acc = piece if acc is None else acc + piece
    for k, (r0, r1) in enumerate(((1, 3), (0, 2), (4, 4))):
        part[k] = jnp.concatenate(
            [acc[r : r + 1, i * HEAD : (i + 1) * HEAD] for r in (r0, r1) for i in range(nc)], axis=0
        ).astype(BF16)
    pl.semaphore_wait(barrier, nsp + ntp - 2)
    loads[7].wait()
    mcopies = [
        [
            remote(
                part.at[cut], mgath.at[d - 1, cut], msend, mrecv.at[e],
                at_sp(lax.rem(sp + d, nsp)),
            )
            for d in range(1, nsp)
        ]
        for e, cut in enumerate((pl.ds(0, 1), pl.ds(1, 2)))
    ]
    for cp in mcopies[0]:
        cp.start()
    for d in range(1, nx):
        lat_copy(d, 0, x).start()
    for cp in mcopies[1]:
        cp.start()
    own = remote(latb.at[mine], latb.at[mine], psend, precv, partner)
    own.start()
    for i in (4, 5, 6, 8):
        loads[i].start()

    def measure_rows(src, row0, st0, count):
        step = 16

        @pl.loop(0, count // step)
        def _(i):
            v = src[pl.ds(row0 + i * step, step), :]
            parts = [None] * 4
            for j in range(width // HEAD):
                t = v[:, j * HEAD : (j + 1) * HEAD].astype(F32)
                parts[j % 4] = t if parts[j % 4] is None else parts[j % 4] + t
            st_mean[pl.ds(st0 + i * step, step), :] = (parts[0] + parts[1]) + (parts[2] + parts[3])

        whole = pl.ds(st0, count)
        mean = jnp.sum(st_mean[whole, :], axis=-1, keepdims=True) * (1.0 / width)
        st_mean[whole, :] = jnp.broadcast_to(mean, (count, HEAD))

        @pl.loop(0, count // step)
        def _(i):
            v = src[pl.ds(row0 + i * step, step), :]
            m = st_mean[pl.ds(st0 + i * step, step), :]
            parts = [None] * 4
            for j in range(width // HEAD):
                t = v[:, j * HEAD : (j + 1) * HEAD].astype(F32) - m
                t = t * t
                parts[j % 4] = t if parts[j % 4] is None else parts[j % 4] + t
            st_rstd[pl.ds(st0 + i * step, step), :] = (parts[0] + parts[1]) + (parts[2] + parts[3])

        var = jnp.sum(st_rstd[whole, :], axis=-1, keepdims=True) * (1.0 / width)
        st_rstd[whole, :] = jnp.broadcast_to(lax.rsqrt(var + EPS), (count, HEAD))

    def shift_rows(src, row0, st0, dst, dst0, count, r_shift, r_scale):
        step = min(32, count)
        rep = step // 8

        @pl.loop(0, count // step)
        def _(i):
            srow = pl.ds(st0 + i * step, step)
            m = st_mean[srow, :]
            r = st_rstd[srow, :]
            for j in range(width // HEAD):
                cols = slice(j * HEAD, (j + 1) * HEAD)
                v = src[pl.ds(row0 + i * step, step), cols].astype(F32)
                v = (v - m) * r
                sc = jnp.concatenate([mod[r_scale, :, cols]] * rep, axis=0)
                sh = jnp.concatenate([mod[r_shift, :, cols]] * rep, axis=0)
                dst[pl.ds(dst0 + i * step, step), cols] = (v * sc + sh).astype(BF16)

    base = pl.multiple_of(x * chip, chip)
    measure_rows(latb, pl.multiple_of(tp * rows, rows), pl.multiple_of(c * rows, rows), rows)
    loads[3].wait()
    measure_rows(ctxb, 0, chip, crows)
    tcopies = [
        [
            remote(
                tslots.at[tp, cut], tslots.at[tp, cut], tsend, trecv.at[e],
                at_tp(lax.rem(tp + d, ntp)),
            )
            for d in range(1, ntp)
        ]
        for e, cut in enumerate((pl.ds(0, 1), pl.ds(1, 2)))
    ]
    for e, cut in enumerate((slice(0, 1), slice(1, 3))):
        acc = part[cut].astype(F32)
        arrivals = mgath.at[:, cut]
        remote(arrivals, arrivals, msend, mrecv.at[e], partner).wait_recv()
        for d in range(1, nsp):
            acc = acc + mgath[d - 1, cut].astype(F32)
        tslots[tp, cut] = acc.astype(BF16)
        for cp in tcopies[e]:
            cp.start()
        if e == 0:
            own.wait_recv()
        for d in range(1, nx):
            for k in (1,) if e == 0 else range(2, len(steps)):
                lat_copy(d, k, x).start()
    measure_rows(latb, pl.multiple_of((x * CORES + oc) * rows, rows), pl.multiple_of(oc * rows, rows), rows)

    def spread(e, picks):
        others = tslots.at[pl.ds(0, ntp - 1), slice(0, 1) if e == 0 else slice(1, 3)]
        remote(others, others, tsend, trecv.at[e], partner).wait_recv()
        for k, first, r, bump in picks:
            for t in range(ntp):
                v = tslots[t, k].astype(F32)
                for i in range(nc):
                    row = v[first * nc + i : first * nc + i + 1] + bump
                    mod[r, :, t * mcols + i * HEAD : t * mcols + (i + 1) * HEAD] = jnp.broadcast_to(row, (8, HEAD))

    spread(0, ((0, 0, 1, 0.0), (0, 1, 3, 1.0)))
    loads[4].wait()
    loads[5].wait()

    def ctx_block(h, o):
        return (ctxk if h == 0 else ctxv).at[pl.ds(pl.multiple_of(o * crows, crows), crows)]

    def z_copy(way, k, h, o):
        to = jnp.clip(z + (1 if way == 0 else -1), 0, nz - 1) * ny + y
        return remote(ctx_block(h, o), ctx_block(h, o), zsend.at[way, k], zrecv.at[way, k, h], at_sp(to))

    def y_copy(d, h, o):
        to = z * ny + lax.rem(y + d, ny)
        return remote(
            ctx_block(h, o), ctx_block(h, o), ysend.at[d - 1, h], yrecv.at[d - 1, h], at_sp(to)
        )

    def arrived(k, way):
        return (z >= k) if way == 0 else (z + k < nz)

    def goes_on(way):
        return (z + 1 < nz) if way == 0 else (z >= 1)

    def origin(k, way):
        return z - k if way == 0 else z + k

    def pass_on(k, way, h, o, act):
        if k < nz - 1:
            @pl.when(goes_on(way))
            def _():
                act(z_copy(way, k, h, o))
        if k > 0 or way == 0:
            for d in range(1, ny):
                act(y_copy(d, h, o))

    def each_block(k, fn):
        for way in range(2):
            if k == 0:
                fn(way, sp)
            else:
                @pl.when(arrived(k, way))
                def _():
                    fn(way, origin(k, way) * ny + y)

    def relay(k, h):
        def one(way, o):
            if k > 0:
                z_copy(way, k - 1, h, o).wait_recv()
            pass_on(k, way, h, o, lambda cp: cp.start())

        each_block(k, one)

    shift_rows(ctxb, 0, chip, mb, 0, crows, 1, 3)
    crow = pl.ds(pl.multiple_of(sp * crows, crows), crows)
    for w, dst in ((wk, ctxk), (wv, ctxv)):
        dst[crow, :] = jnp.dot(mb[0:crows, :], w[...], preferred_element_type=F32).astype(BF16)
    for h in range(2):
        relay(0, h)
    events = [(k, h) for k in range(1, nz) for h in range(2)]

    def poll(n):
        for _ in range(n):
            if events:
                k, h = events.pop(0)
                relay(k, h)

    spread(1, ((1, 0, 0, 0.0), (1, 1, 2, 1.0), (2, 0, 4, 0.0)))

    lane = lax.broadcasted_iota(jnp.int32, (1, HEAD), 1)
    low = lax.rem(lane, HEAD // 2) < HEAD // 4

    def turn(v, row0, count, factor):
        v = v.astype(BF16).astype(F32)
        swapped = jnp.where(low, pltpu.roll(v, HEAD - HEAD // 4, 1), pltpu.roll(v, HEAD // 4, 1))
        r = v * cos_t[pl.ds(row0, count), :] + swapped * sin_t[pl.ds(row0, count), :]
        return (r * factor).astype(BF16)

    def project(segments):
        total = sum(n for _, n in segments)
        qf = HEAD ** (-0.5) * LOG2E
        for w, cols, kind in ((wq, qc, 0), (wk, kc, 1), (wv, kc, 2)):
            tile = min(256, cols)
            for n0 in range(0, cols, tile):
                r = jnp.dot(mb[0:total, :], w[:, n0 : n0 + tile], preferred_element_type=F32)
                off = 0
                for row0, n in segments:
                    for h in range(0, tile, HEAD):
                        v = r[off : off + n, h : h + HEAD]
                        if kind == 0:
                            q_s[pl.ds(row0, n), n0 + h : n0 + h + HEAD] = turn(v, row0, n, qf)
                        elif kind == 1:
                            kv[pl.ds(row0 + SIDE, n), n0 + h : n0 + h + HEAD] = turn(v, row0, n, 1.0)
                        else:
                            kv[pl.ds(row0 + SIDE, n), kc + n0 + h : kc + n0 + h + HEAD] = v.astype(BF16)
                    off += n

    loads[6].wait()
    shift_rows(latb, base, 0, mb, 0, chip, 0, 2)
    project([(base, chip)])
    left = at_sp(lax.rem(sp + nsp - 1, nsp))
    right = at_sp(lax.rem(sp + 1, nsp))
    to_left = remote(kv.at[pl.ds(SIDE, SIDE)], kv.at[pl.ds(SIDE + tokens, SIDE)], hsend, hrecv.at[0], left)
    to_right = remote(kv.at[pl.ds(tokens, SIDE)], kv.at[pl.ds(0, SIDE)], hsend, hrecv.at[1], right)

    def gather(d, quarter):
        for i, k in enumerate(fresh[quarter]):
            lat_copy(d, k, from_x(d)).wait_recv()
            fwd_copy(d, k, c).start()
            if i == 0 and d == 1:
                poll(2)

    def normalize(d, quarter, dst0):
        for k in fresh[quarter]:
            fwd_copy(d, k, oc).wait_recv()
        n = units // 2 * UNIT
        row0 = pl.multiple_of(from_x(d) * chip + quarter * n, n)
        measure_rows(latb, row0, dst0, n)
        shift_rows(latb, row0, dst0, mb, dst0, n, 0, 2)

    def project_chip(d, quarter, count):
        n = units // 2 * UNIT
        project([(pl.multiple_of(from_x(d) * chip + quarter * n, n), count * n)])

    def wait_context():
        poll(len(events))
        for d in range(1, ny):
            for h, ref in enumerate((ctxk, ctxv)):
                column = ref.at[pl.ds(0, nz * crows)]
                remote(column, column, ysend.at[d - 1, h], yrecv.at[d - 1, h], partner).wait_recv()

    def attend(r0, n, dst0):
        band = n + 2 * SIDE
        key_i = lax.broadcasted_iota(jnp.int32, (n, band), 1)
        gap = key_i - lax.broadcasted_iota(jnp.int32, (n, band), 0)
        kpos = key_i + (sp * tokens + r0 - SIDE)
        valid = (gap >= 0) & (gap <= 2 * SIDE) & (kpos >= 0) & (kpos < tokens * nsp)
        bias = jnp.where(valid, 0.0, MASKED)
        bias = jnp.concatenate([bias] * group, axis=0)
        for h in range(kv_heads):
            heads = [h * group + i for i in range(group)]
            q = jnp.concatenate([q_s[pl.ds(r0, n), j * HEAD : (j + 1) * HEAD] for j in heads], axis=0)
            kb = kv[pl.ds(r0, band), h * HEAD : (h + 1) * HEAD]
            vb = kv[pl.ds(r0, band), kc + h * HEAD : kc + (h + 1) * HEAD]
            kx = ctxk[:, h * HEAD : (h + 1) * HEAD]
            vx = ctxv[:, h * HEAD : (h + 1) * HEAD]
            dims = (((1,), (1,)), ((), ()))
            sb = lax.dot_general(q, kb, dims, preferred_element_type=F32) + bias
            sx = lax.dot_general(q, kx, dims, preferred_element_type=F32)
            snk = jnp.concatenate(
                [jnp.full((n, 1), sink[tp * (qc // HEAD) + j], F32) for j in heads], axis=0
            ) * LOG2E
            top = jnp.maximum(
                jnp.maximum(jnp.max(sb, axis=-1, keepdims=True), jnp.max(sx, axis=-1, keepdims=True)), snk
            )
            eb = jnp.exp2(sb - top)
            ex = jnp.exp2(sx - top)
            den = jnp.sum(eb, axis=-1, keepdims=True) + jnp.sum(ex, axis=-1, keepdims=True) + jnp.exp2(snk - top)
            o = jnp.dot(eb.astype(BF16), vb, preferred_element_type=F32) + jnp.dot(
                ex.astype(BF16), vx, preferred_element_type=F32
            )
            o = (o / den).astype(BF16)
            for i, j in enumerate(heads):
                att[pl.ds(dst0, n), j * HEAD : (j + 1) * HEAD] = o[i * n : (i + 1) * n]

    tile_cols = width // TILES
    half = TILES // CORES
    jobs = ((0, rows // 2, 0), (rows // 2, rows, 0), (rows, chip, 1))

    def cols_of(n):
        return slice(n * tile_cols, (n + 1) * tile_cols)

    def dyn_cols(n):
        return pl.ds(pl.multiple_of(n * tile_cols, tile_cols), tile_cols)

    def d_copy(g, j, i):
        a, b, _ = jobs[j]
        span = pl.ds(a, b - a)
        return remote(away.at[g, i, span], prcv.at[g, i, span], dsend, drecv.at[g, j, i], partner)

    def x_copy(g, j, i, sender):
        a, b, owner = jobs[j]
        xo = lax.rem(x + 1 + g, nx)
        return remote(
            comb.at[g, i, pl.ds(a, b - a)], xrcv.at[g, sender * half + i, pl.ds(a - owner * rows, b - a)],
            xsend, xrecv.at[g, j - owner * 2, sender * half + i], at_tp(xo * CORES + owner),
        )

    def chip_job(g, j):
        a, b, _ = jobs[j]
        xo = lax.rem(x + 1 + g, nx)
        attend(pl.multiple_of(xo * chip + a, UNIT), b - a, a)
        for ref, core in ((away, oc), (keep, c)):
            for i in range(half):
                ref[g, i, a:b] = jnp.dot(
                    att[a:b, :], wo[:, dyn_cols(core * half + i)], preferred_element_type=F32
                ).astype(BF16)
                if ref is away:
                    d_copy(g, j, i).start()

    def combine(g, j):
        a, b, _ = jobs[j]
        for i in range(half):
            d_copy(g, j, i).wait_recv()
            comb[g, i, a:b] = (keep[g, i, a:b].astype(F32) + prcv[g, i, a:b].astype(F32)).astype(BF16)
            x_copy(g, j, i, c).start()

    def halo(first):
        @pl.when((x == 0) if first else (x != 0))
        def _():
            to_left.start()

        @pl.when((x == nx - 1) if first else (x != nx - 1))
        def _():
            to_right.start()

    def wait_halo(first):

        @pl.when((x != 0) if first else (x == 0))
        def _():
            to_right.wait_recv()

        @pl.when((x != nx - 1) if first else (x == nx - 1))
        def _():
            to_left.wait_recv()

    for d in range(1, nx):
        for quarter in range(4):
            gather(d, quarter)
            if quarter == 3 and nx == 2:
                combine(0, 0)
            normalize(d, quarter, quarter * (units // 2 * UNIT) if quarter < 2 else 0)
            if quarter > 0:
                project_chip(d, max(quarter - 1, 0) if quarter == 1 else quarter, 2 if quarter == 1 else 1)
            if quarter == 1 and d == 1:
                halo(True)
            if quarter == 2 and nx == 2:
                wait_context()
                wait_halo(True)
                loads[8].wait()
                loads[11].wait()
                chip_job(0, 0)
    halo(False)
    if nx > 2:
        wait_context()
        wait_halo(True)
        loads[8].wait()
        loads[11].wait()
    for g in range(nx - 1):
        for j in range(1 if nx == 2 else 0, len(jobs)):
            chip_job(g, j)
            combine(g, j)
    wait_halo(False)

    @pl.loop(0, 2)
    def _(u):
        attend(
            pl.multiple_of(base + lax.rem(oc + u, 2) * rows, rows), rows, pl.multiple_of(u * rows, rows)
        )

    own_copy = remote(stage.at[:, pl.ds(0, rows)], orcv, osend, orecv, partner)
    for n in range(TILES):
        stage[n] = jnp.dot(att[...], wo[:, cols_of(n)], preferred_element_type=F32).astype(BF16)
    own_copy.start()
    own_copy.wait_recv()

    def finish(j):
        a, b, owner = jobs[j]
        span = slice(a - owner * rows, b - owner * rows)
        for i in range(half):
            for sender in range(CORES):
                n = sender * half + i
                part_rows = slice(rows + span.start, rows + span.stop)
                total = stage[n, part_rows].astype(F32) + orcv[n, span].astype(F32)
                for g in range(nx - 1):
                    x_copy(g, j, i, sender).wait_recv()
                    total = total + xrcv[g, n, span].astype(F32)
                rows_of = pl.ds(pl.multiple_of(tp * rows, rows) + span.start, b - a)
                out[span, cols_of(n)] = (
                    latb[rows_of, cols_of(n)].astype(F32) + mod[4, 0:1, cols_of(n)] * total
                ).astype(BF16)

    for owner in range(CORES):
        @pl.when(c == owner)
        def _():
            for j in range(len(jobs)):
                if jobs[j][2] == owner:
                    finish(j)


    def sent(ref, sem):
        remote(ref, ref, sem, sem, partner).wait_send()

    own.wait_send()
    own_copy.wait_send()
    sent(mgath, msend)
    sent(tslots.at[pl.ds(0, ntp - 1)], tsend)
    sent(kv.at[pl.ds(0, 2 * SIDE)], hsend)
    for k in range(nz - 1):
        for way in range(2):
            @pl.when(goes_on(way) & (arrived(k, way) if k > 0 else True))
            def _():
                sent(ctxk.at[pl.ds(0, 2 * crows)], zsend.at[way, k])
    for d in range(1, ny):
        for h in range(2):
            sent(ctxk.at[pl.ds(0, nz * crows)], ysend.at[d - 1, h])
    for d in range(1, nx):
        sent(latb.at[pl.ds(0, rows)], lsend.at[d - 1])
        sent(latb.at[pl.ds(0, rows)], fsend.at[d - 1])
    sent(prcv, dsend)
    sent(comb, xsend)


def shards(lat, ctx, cond, ctx_cond, w_shift, w_scale, w_gate, w_q, w_k, w_v, w_o, sink):
    nsp = lax.axis_size("sp")
    ntp = lax.axis_size("tp")
    nx = ntp // CORES
    ny = grid_y(nsp)
    nz = nsp // ny
    hops = max(nz - 1, 1)
    rows, width = lat.shape
    crows = ctx.shape[0]
    tokens = rows * ntp
    qc = w_q.shape[1]
    kc = w_k.shape[1]
    mrows, mcols = w_shift.shape
    nc2 = 2 * (mcols // HEAD)
    _, steps, _ = unit_plan(rows)
    half = TILES // CORES
    any_ = pl.BlockSpec(memory_space=pl.ANY)
    vmem = pl.BlockSpec(memory_space=pltpu.VMEM)
    dma = pltpu.SemaphoreType.DMA
    V = pltpu.VMEM
    return pl.pallas_call(
        functools.partial(body, nsp, ntp),
        out_shape=pltpu.VMEM((rows, width), BF16),
        in_specs=[any_] * 12,
        out_specs=vmem,
        scratch_shapes=[
            V((tokens, HEAD), F32), V((tokens, HEAD), F32), V((CORES * rows + crows, HEAD), F32),
            V((CORES * rows + crows, HEAD), F32), V((ntp, 3, nc2, HEAD), BF16),
            V((3, mrows, mcols), BF16), V((width, qc), BF16), V((width, kc), BF16), V((width, kc), BF16),
            V((qc, width), BF16), V((ntp * rows, width), BF16), V((crows, width), BF16),
            V((max(CORES * rows, crows), width), BF16), V((3, nc2, HEAD), BF16), V((nsp - 1, 3, nc2, HEAD), BF16),
            V((5, 8, width), F32), V((nsp * crows, kc), BF16), V((nsp * crows, kc), BF16), V((tokens, qc), BF16),
            V((tokens + 2 * SIDE, 2 * kc), BF16), V((2 * rows, qc), BF16),
            V((nx - 1, half, CORES * rows, width // TILES), BF16), V((nx - 1, half, CORES * rows, width // TILES), BF16),
            V((nx - 1, half, CORES * rows, width // TILES), BF16), V((nx - 1, half, CORES * rows, width // TILES), BF16),
            V((nx - 1, TILES, rows, width // TILES), BF16), V((TILES, 2 * rows, width // TILES), BF16),
            V((TILES, rows, width // TILES), BF16), V((2, width), F32), pltpu.SMEM(sink.shape, F32),
            dma((12,)), dma, dma((2,)), dma, dma((2,)),
            dma((nx - 1,)), dma((nx - 1, len(steps))), dma((nx - 1,)), dma((nx - 1, len(steps))), dma, dma,
            dma((2, hops)), dma((2, hops, 2)), dma((max(ny - 1, 1), 2)), dma((max(ny - 1, 1), 2)),
            dma, dma((2,)), dma, dma((nx - 1, 3, half)), dma, dma((nx - 1, 2, TILES)), dma, dma,
        ],
        compiler_params=pltpu.CompilerParams(
            collective_id=0, has_side_effects=True, vmem_limit_bytes=60 * 1024 * 1024
        ),
    )(
        lat, ctx, cond, ctx_cond,
        w_shift, w_scale, w_gate, w_q, w_k, w_v, w_o, sink,
    )


def solution(mesh):
    in_specs = (
        P(("sp", "tp"), None), P("sp", None), P(), P(), P("sp", "tp"), P("sp", "tp"), P("sp", "tp"),
        P(None, "tp"), P(None, "tp"), P(None, "tp"), P("tp", None), P(),
    )
    return jax.shard_map(
        shards, mesh=mesh, in_specs=in_specs, out_specs=P(("sp", "tp"), None), check_vma=False
    )
```

time: 68.1 us -> 63.2 us (0.928)
  Pallas kernels: 66.3 us -> 62 us
    pallas_call x1, Pallas kernels: 66.3 us -> 62 us  [shards(): pl.pallas_call(functools.partial(body, nsp, ntp), out_shape=pltpu.VMEM((r...]
where the time goes in v2:
time: 63.2 us; the launch traced here: 63 us
  Pallas kernels  62 us (98%)
  local copies, waits for them, and re-layouts  0.97 us (2%)
    pallas_call x1, Pallas kernels, shards(): pl.pallas_call(functools.partial(body, nsp, ntp), out_shape=pltpu.VMEM((r...  62 us

profile of v2, /device:TPU:1, one launch (start us, length us, event | category | flops | bytes accessed | tf_op | source)
XLA Modules:
  0.0 63.0 jit_solution(8374533356432251960)
XLA Ops:
  0.0 62.0 %shard_map.118 = bf16[128,4096]{1,0:T(8,128)(2,1)S(1)} custom-call(bf16[128,4096]{1,0:T(8,128)(2,1)} %lat.1, bf16[128,4096]{1,0:T(8,128)(2,1)} %ctx.1, f32[4096]{0:T(1024)} %cond.1, f32[4096]{0:T(1024)} %ctx_cond.1, bf16[512,1024]{1,0:T(8,128)(2,1)} %w_shift.1, bf16[512,1024]{1,0:T(8,128)(2,1)} %w_scale.1, bf16[512,1024]{1,0:T(8,128)(2,1)} %w_gate.1, ...), custom_call_target="tpu_custom_call" | custom-call | tf_op jit(solution)/shard_map/pallas_call | solution.py:598
  62.0 1.0 %copy.14 = bf16[128,4096]{1,0:T(8,128)(2,1)} copy(bf16[128,4096]{1,0:T(8,128)(2,1)S(1)} %shard_map.118) | data formatting | bytes 2097152
